TPU v7x, 32 devices: a whole 2x2x4 slice. The times are simulated.
32 devices in a mesh: dp: 4 (over y, x), kv: 4 (over z), tp: 2 (over core).
Axes of the slice: x: 2, y: 2, z: 4, core: 2. Of those that a mesh axis runs over, the one named last changes fastest.
Arguments:
- tokens: bfloat16 [128, 2048], P('dp', ('kv', 'tp')), may hold values from -60 to 60
- first_norm_gain: float32 [2048], replicated, may hold values from 0.1 to 1.9
- first_gate_weight: bfloat16 [2048, 5632], P(None, ('kv', 'tp')), may hold values from -0.125 to 0.125
- first_up_weight: bfloat16 [2048, 5632], P(None, ('kv', 'tp')), may hold values from -0.125 to 0.125
- first_down_weight: bfloat16 [5632, 2048], P(('kv', 'tp')), may hold values from -0.109375 to 0.109375
- mixer_norm_gain: float32 [2048], replicated, may hold values from 0.1 to 1.9
- query_weight: bfloat16 [2048, 1024], P('kv', 'tp'), may hold values from -0.125 to 0.125
- key_weight: bfloat16 [2048, 1024], P('kv', 'tp'), may hold values from -0.125 to 0.125
- value_weight: bfloat16 [2048, 1024], P('kv', 'tp'), may hold values from -0.125 to 0.125
- output_gate_weight: bfloat16 [2048, 1024], P('kv', 'tp'), may hold values from -0.125 to 0.125
- strength_weight: bfloat16 [2048, 8], replicated, may hold values from -0.125 to 0.125
- decay_weight: bfloat16 [2048, 8], replicated, may hold values from -0.125 to 0.125
- head_decay_log: float32 [8], replicated, may hold values from 0 to 2.77
- decay_input_bias: float32 [8], replicated, may hold values from -4 to 0
- decay_extra_log: float32 [128, 8], P(('dp', 'kv'), 'tp'), may hold values from -0.7 to 0
- head_norm_gain: float32 [128], replicated, may hold values from 0.1 to 1.9
- state: float32 [128, 8, 128, 128], P(('dp', 'kv'), 'tp'), may hold values from -0.6 to 0.6
- mixer_output_weight: bfloat16 [1024, 2048], P('tp', 'kv'), may hold values from -0.1875 to 0.1875
- second_norm_gain: float32 [2048], replicated, may hold values from 0.1 to 1.9
- second_gate_weight: bfloat16 [2048, 5632], P(None, ('kv', 'tp')), may hold values from -0.125 to 0.125
- second_up_weight: bfloat16 [2048, 5632], P(None, ('kv', 'tp')), may hold values from -0.125 to 0.125
- second_down_weight: bfloat16 [5632, 2048], P(('kv', 'tp')), may hold values from -0.109375 to 0.109375
Outputs:
- layer_out: bfloat16 [128, 2048], P('dp', ('kv', 'tp'))
- new_state: float32 [128, 8, 128, 128], P(('dp', 'kv'), 'tp')
All inputs are finite; a program needn't handle non-finite values.
Results may differ from a plain program's by a relative error of at most 0.014.
Values may be sent and summed in bfloat16 or wider, within the bound.
A program may use at most 64 MiB of HBM per device.

v0:
```python
import jax
import jax.numpy as jnp
from jax import lax
from jax.sharding import PartitionSpec as P

EPS = 1e-06


def row_scale(values):
    return lax.rsqrt(jnp.mean(values * values, axis=-1, keepdims=True) + EPS)


def unit_rows(values):
    return values * lax.rsqrt(jnp.sum(values * values, axis=-1, keepdims=True) + EPS)


def block_terms(row_data, gain_vec, w_gate, w_up, w_down):
    rows32 = row_data.astype(jnp.float32)
    normed = (rows32 * row_scale(rows32) * gain_vec).astype(jnp.bfloat16)
    gate_pre = jnp.dot(normed, w_gate, preferred_element_type=jnp.float32)
    upward = jnp.dot(normed, w_up, preferred_element_type=jnp.float32)
    hidden = (jax.nn.silu(gate_pre) * upward).astype(jnp.bfloat16)
    return jnp.dot(hidden, w_down, preferred_element_type=jnp.float32)


def delta_step(
    query_vec, key_vec, value_vec, gate_vals, beta_gate, head_decay_rate, state, head_norm_gain
):
    recalled = jnp.einsum("shd,shde->she", key_vec, state, precision=lax.Precision.HIGHEST)
    correction = beta_gate[..., None] * (value_vec - head_decay_rate[..., None] * recalled)
    new_state = (
        head_decay_rate[..., None, None] * state + key_vec[..., :, None] * correction[..., None, :]
    )
    read_out = jnp.einsum("shd,shde->she", query_vec, new_state, precision=lax.Precision.HIGHEST)
    normed = read_out * row_scale(read_out) * head_norm_gain
    return (normed * jax.nn.silu(gate_vals), new_state)


def shards(
    tokens,
    first_norm_gain,
    first_gate_weight,
    first_up_weight,
    first_down_weight,
    mixer_norm_gain,
    query_weight,
    key_weight,
    value_weight,
    output_gate_weight,
    strength_weight,
    decay_weight,
    head_decay_log,
    decay_input_bias,
    decay_extra_log,
    head_norm_gain,
    state,
    mixer_output_weight,
    second_norm_gain,
    second_gate_weight,
    second_up_weight,
    second_down_weight,
):
    batch_rows, columns = tokens.shape
    kv_index = lax.axis_index("kv")
    tp_index = lax.axis_index("tp")
    own_block = kv_index * lax.axis_size("tp") + tp_index
    seq_dev, heads_dev, head_size = (state.shape[0], state.shape[1], state.shape[2])
    kv_width = query_weight.shape[0]
    head_cols = heads_dev * head_size
    model_width = mixer_norm_gain.shape[0]
    rows_all = lax.all_gather(tokens, ("kv", "tp"), axis=1, tiled=True)
    ffn_terms = block_terms(
        rows_all, first_norm_gain, first_gate_weight, first_up_weight, first_down_weight
    )
    share_sum = lax.psum_scatter(
        ffn_terms.astype(jnp.bfloat16), ("kv", "tp"), scatter_dimension=1, tiled=True
    ).astype(jnp.float32)
    first_rows = (tokens.astype(jnp.float32) + 0.5 * share_sum).astype(jnp.bfloat16)
    first32 = first_rows.astype(jnp.float32)
    kv_block = lax.all_gather(first_rows, "tp", axis=1, tiled=True)
    own_gain = lax.dynamic_slice_in_dim(mixer_norm_gain, own_block * columns, columns)
    own_scaled = (first32 * own_gain).astype(jnp.bfloat16)
    beta_rows = lax.dynamic_slice_in_dim(strength_weight, own_block * columns, columns, 0)
    decay_rows = lax.dynamic_slice_in_dim(decay_weight, own_block * columns, columns, 0)
    squares, beta_pre, decay_logits = lax.psum(
        (
            jnp.sum(first32 * first32, axis=1),
            jnp.dot(own_scaled, beta_rows, preferred_element_type=jnp.float32),
            jnp.dot(own_scaled, decay_rows, preferred_element_type=jnp.float32),
        ),
        ("kv", "tp"),
    )
    row_factor = lax.rsqrt(squares / model_width + EPS)
    block_gain = lax.dynamic_slice_in_dim(mixer_norm_gain, kv_index * kv_width, kv_width)
    block_scaled = (kv_block.astype(jnp.float32) * block_gain).astype(jnp.bfloat16)
    projected = lax.psum_scatter(
        jnp.concatenate(
            [
                jnp.dot(block_scaled, weight, preferred_element_type=jnp.float32)
                for weight in (query_weight, key_weight, value_weight, output_gate_weight)
            ],
            axis=1,
        ).astype(jnp.bfloat16),
        "kv",
        scatter_dimension=0,
        tiled=True,
    ).astype(jnp.float32)
    own_rows = kv_index * seq_dev
    own_factor = lax.dynamic_slice_in_dim(row_factor, own_rows, seq_dev)[:, None]
    projected = projected * own_factor

    def split_heads(role_index):
        return projected[:, role_index * head_cols : (role_index + 1) * head_cols].reshape(
            seq_dev, heads_dev, head_size
        )

    query_vec = unit_rows(jax.nn.silu(split_heads(0))) * head_size ** (-0.5)
    key_vec = unit_rows(jax.nn.silu(split_heads(1)))
    value_vec = jax.nn.silu(split_heads(2))
    gate_vals = split_heads(3)
    head_start = tp_index * heads_dev

    def local_gate_values(values):
        own_seqs = lax.dynamic_slice_in_dim(values, own_rows, seq_dev, 0)
        return lax.dynamic_slice_in_dim(own_seqs, head_start, heads_dev, 1) * own_factor

    beta_gate = jax.nn.sigmoid(local_gate_values(beta_pre))
    decay_log_term = lax.dynamic_slice_in_dim(head_decay_log, head_start, heads_dev)
    decay_offset_term = lax.dynamic_slice_in_dim(decay_input_bias, head_start, heads_dev)
    head_decay_rate = jnp.exp(
        decay_extra_log
        - jnp.exp(decay_log_term)
        * jax.nn.softplus(local_gate_values(decay_logits) + decay_offset_term)
    )
    heads_f32, new_state = delta_step(
        query_vec, key_vec, value_vec, gate_vals, beta_gate, head_decay_rate, state, head_norm_gain
    )
    heads_out = heads_f32.reshape(seq_dev, head_cols).astype(jnp.bfloat16)
    mixer_terms = jnp.dot(
        lax.all_gather(heads_out, "kv", axis=0, tiled=True),
        mixer_output_weight,
        preferred_element_type=jnp.float32,
    )
    mixer_sum = lax.psum_scatter(
        mixer_terms.astype(jnp.bfloat16), "tp", scatter_dimension=1, tiled=True
    ).astype(jnp.float32)
    second_rows = (first32 + mixer_sum).astype(jnp.bfloat16)
    rows_last = lax.all_gather(second_rows, ("kv", "tp"), axis=1, tiled=True)
    last_terms = block_terms(
        rows_last, second_norm_gain, second_gate_weight, second_up_weight, second_down_weight
    )
    last_sum = lax.psum_scatter(
        last_terms.astype(jnp.bfloat16), ("kv", "tp"), scatter_dimension=1, tiled=True
    ).astype(jnp.float32)
    layer_out = (second_rows.astype(jnp.float32) + 0.5 * last_sum).astype(jnp.bfloat16)
    return (layer_out, new_state)


def solution(mesh):
    placed = (
        P("dp", ("kv", "tp")),
        P(),
        P(None, ("kv", "tp")),
        P(None, ("kv", "tp")),
        P(("kv", "tp"), None),
        P(),
        P("kv", "tp"),
        P("kv", "tp"),
        P("kv", "tp"),
        P("kv", "tp"),
        P(),
        P(),
        P(),
        P(),
        P(("dp", "kv"), "tp"),
        P(),
        P(("dp", "kv"), "tp", None, None),
        P("tp", "kv"),
        P(),
        P(None, ("kv", "tp")),
        P(None, ("kv", "tp")),
        P(("kv", "tp"), None),
    )
    return jax.shard_map(
        shards,
        mesh=mesh,
        in_specs=placed,
        out_specs=(P("dp", ("kv", "tp")), P(("dp", "kv"), "tp", None, None)),
        check_vma=False,
    )
```

profile of v0, /device:TPU:0, one launch (start us, length us, event | category | flops | bytes accessed | tf_op | source)
XLA Modules:
  0.0 181.2 jit_solution(4792796293112144642)
XLA Ops:
  7.2 16.1 %all_gather.12 = bf16[32,2048]{1,0:T(8,128)(2,1)S(1)} all-gather(bf16[32,256]{1,0:T(8,128)(2,1)} %param.22), channel_id=1, replica_groups=mesh['dp'=4,'kv'=4,'tp'=2] {'kv','tp'}, dimensions={1}, use_global_device_ids=true | all-gather | bytes 147456 | tf_op jit(solution)/shard_map/all_gather | solution.py:71
  24.0 3.4 %fusion.26 = f32[32,704]{1,0:T(8,128)} fusion(bf16[2048,704]{0,1:T(8,128)(2,1)} %param.24, bf16[32,2048]{1,0:T(8,128)(2,1)S(1)} %all_gather.12, f32[2048]{0:T(1024)} %param.23, f32[32]{0:T(128)S(1)} %add_rsqrt_fusion.5), kind=kOutput, calls=%fused_computation.41 | convolution fusion | flops 92536832 | bytes 3113088 | tf_op jit(solution)/shard_map/dot_general | solution.py:20
  27.4 4.3 %convolution_convert_fusion.1 = bf16[32,2048]{1,0:T(8,128)(2,1)} fusion(bf16[704,2048]{1,0:T(8,128)(2,1)S(1)} %copy-done, bf16[2048,704]{0,1:T(8,128)(2,1)} %param.25, f32[32,704]{1,0:T(8,128)} %fusion.26, bf16[32,2048]{1,0:T(8,128)(2,1)S(1)} %all_gather.12, f32[2048]{0:T(1024)} %param.23, f32[32]{0:T(128)} %copy-done.8), kind=kOutput, calls=%fused_computation.1 | convolution fusion | flops 185012224 | bytes 6127744 | tf_op jit(solution)/shard_map/dot_general | solution.py:23
  34.8 28.7 %reduce-scatter.5.cloned.1.call-done = bf16[32,256]{1,0:T(8,128)(2,1)} async-done(((bf16[32,2048]{1,0:T(8,128)(2,1)}), bf16[32,256]{1,0:T(8,128)(2,1)}) %reduce-scatter.5.cloned.1.call-update) | async-done | bytes 16400 | tf_op jit(solution)/shard_map/reduce_scatter | solution.py:75
  63.5 0.8 fusion.28
  64.3 1.8 %all_gather.13 = bf16[32,512]{1,0:T(8,128)(2,1)S(1)} all-gather(bf16[32,256]{1,0:T(8,128)(2,1)S(1)} %get-tuple-element.8), channel_id=1, replica_groups=mesh['dp'=4,'kv'=4,'tp'=2] {'tp'}, dimensions={1}, use_global_device_ids=true | all-gather | bytes 49152 | tf_op jit(solution)/shard_map/all_gather | solution.py:80
  66.2 0.8 fusion.43
  67.0 0.8 fusion.41
  68.0 1.2 convolution_convert_fusion.4
  69.2 1.2 convolution_convert_fusion.3
  70.5 1.3 convolution_convert_fusion.6
  72.5 14.4 %all-reduce = (f32[32]{0:T(128)S(1)}, f32[32,8]{0,1:T(8,128)S(1)}, f32[32,8]{0,1:T(8,128)S(1)}) all-reduce(f32[32]{0:T(128)S(1)} %get-tuple-element.7, f32[32,8]{0,1:T(8,128)S(1)} %fusion.43, f32[32,8]{0,1:T(8,128)S(1)} %fusion.41), channel_id=1, replica_groups=mesh['dp'=4,'kv'=4,'tp'=2] {'kv','tp'}, use_global_device_ids=true, to_apply=%region_4.5 | all-reduce | flops 544 | bytes 4352 | tf_op jit(solution)/shard_map/psum | solution.py:85
  87.1 3.0 %reduce-scatter.7.cloned.1.call-done = bf16[8,2048]{1,0:T(8,128)(2,1)} async-done(((bf16[32,2048]{1,0:T(8,128)(2,1)}), bf16[8,2048]{1,0:T(8,128)(2,1)}) %reduce-scatter.7.cloned.1.call-update) | async-done | bytes 32784 | tf_op jit(solution)/shard_map/reduce_scatter | solution.py:96
  90.1 1.0 convert_multiply_fusion.4
  91.4 3.4 %fusion.39 = f32[8,4,1,128]{3,2,1,0:T(1,128)S(1)} fusion(f32[8,4,128,128]{3,2,1,0:T(8,128)} %param.38, f32[8,4,128,1]{2,0,1,3:T(8,128)S(1)} %fusion.69), kind=kOutput, calls=%fused_computation.62 | convolution fusion | flops 6291456 | bytes 2129920 | tf_op jit(solution)/shard_map/shd,shde->she/dot_general | solution.py:29
  95.7 1.3 copy-done.2
  97.0 1.9 %fusion.37 = f32[8,4,1,128]{3,2,1,0:T(1,128)S(1)} fusion(f32[8,4,128,128]{3,2,1,0:T(8,128)S(1)} %multiply_add_fusion, f32[8,4,128,1]{2,0,1,3:T(8,128)S(1)} %get-tuple-element.9), kind=kOutput, calls=%fused_computation.60 | convolution fusion | flops 6291456 | bytes 2129920 | tf_op jit(solution)/shard_map/shd,shde->she/dot_general | solution.py:34
  99.1 13.1 %all_gather.14 = bf16[32,512]{1,0:T(8,128)(2,1)S(1)} all-gather(bf16[8,512]{1,0:T(8,128)(2,1)S(1)} %fusion.45), channel_id=1, replica_groups=mesh['dp'=4,'kv'=4,'tp'=2] {'kv'}, dimensions={0}, use_global_device_ids=true | all-gather | bytes 40960 | tf_op jit(solution)/shard_map/all_gather | solution.py:140
  113.1 5.8 %reduce-scatter.9.cloned.1.call-done = bf16[32,256]{1,0:T(8,128)(2,1)} async-done(((bf16[32,512]{1,0:T(8,128)(2,1)}), bf16[32,256]{1,0:T(8,128)(2,1)}) %reduce-scatter.9.cloned.1.call-update) | async-done | bytes 16400 | tf_op jit(solution)/shard_map/reduce_scatter | solution.py:144
  119.6 14.3 %all_gather.15 = bf16[32,2048]{1,0:T(8,128)(2,1)S(1)} all-gather(bf16[32,256]{1,0:T(8,128)(2,1)S(1)} %fusion.30), channel_id=1, replica_groups=mesh['dp'=4,'kv'=4,'tp'=2] {'kv','tp'}, dimensions={1}, use_global_device_ids=true | all-gather | bytes 147456 | tf_op jit(solution)/shard_map/all_gather | solution.py:148
  134.0 2.7 %fusion.22 = f32[32,704]{1,0:T(8,128)S(1)} fusion(bf16[2048,704]{0,1:T(8,128)(2,1)} %param.41, bf16[32,2048]{1,0:T(8,128)(2,1)S(1)} %all_gather.15, f32[2048]{0:T(1024)S(1)} %copy-done.6, f32[32]{0:T(128)S(1)} %add_rsqrt_fusion.3), kind=kOutput, calls=%fused_computation.40 | convolution fusion | flops 92536832 | bytes 3113088 | tf_op jit(solution)/shard_map/dot_general | solution.py:20
  136.7 5.1 %convolution_convert_fusion = bf16[32,2048]{1,0:T(8,128)(2,1)} fusion(bf16[704,2048]{1,0:T(8,128)(2,1)} %param.43, bf16[2048,704]{0,1:T(8,128)(2,1)} %param.42, f32[32,704]{1,0:T(8,128)S(1)} %fusion.22, bf16[32,2048]{1,0:T(8,128)(2,1)S(1)} %all_gather.15, f32[2048]{0:T(1024)S(1)} %copy-done.6, f32[32]{0:T(128)S(1)} %add_rsqrt_fusion.3), kind=kOutput, calls=%fused_computation | convolution fusion | flops 185012224 | bytes 6127744 | tf_op jit(solution)/shard_map/dot_general | solution.py:23
  141.9 31.5 %reduce-scatter.11.cloned.1.call-done = bf16[32,256]{1,0:T(8,128)(2,1)} async-done(((bf16[32,2048]{1,0:T(8,128)(2,1)}), bf16[32,256]{1,0:T(8,128)(2,1)}) %reduce-scatter.11.cloned.1.call-update) | async-done | bytes 16400 | tf_op jit(solution)/shard_map/reduce_scatter | solution.py:152
  173.4 1.3 add_convert_fusion
  (54 shorter events, 8.0 us)
Async XLA Ops:
  7.2 20.2 %copy-start = (bf16[704,2048]{1,0:T(8,128)(2,1)S(1)}, bf16[704,2048]{1,0:T(8,128)(2,1)}, u32[]{:S(2)}) copy-start(bf16[704,2048]{1,0:T(8,128)(2,1)} %param.26) | copy-start | bytes 8650756
  7.2 56.3 %reduce-scatter.5.cloned.1.call-start = ((), (), s32[]{:S(2)}) async-start(), calls=%async_computation.4 | async-start | bytes 147456 | tf_op jit(solution)/shard_map/reduce_scatter | solution.py:75
  23.5 0.5 copy-start.8
  27.4 36.2 %copy-start.5 = (bf16[32,256]{1,0:T(8,128)(2,1)S(1)}, bf16[32,256]{1,0:T(8,128)(2,1)}, u32[]{:S(2)}) copy-start(bf16[32,256]{1,0:T(8,128)(2,1)} %param.22) | copy-start | bytes 49156
  27.4 40.4 %copy-start.3 = (bf16[512,512]{1,0:T(8,128)(2,1)S(1)}, bf16[512,512]{1,0:T(8,128)(2,1)}, u32[]{:S(2)}) copy-start(bf16[512,512]{1,0:T(8,128)(2,1)} %param.29) | copy-start | bytes 1572868
  31.7 55.2 %copy-start.7 = (f32[8,4]{0,1:T(4,128)S(1)}, f32[8,4]{0,1:T(4,128)}, u32[]{:S(2)}) copy-start(f32[8,4]{0,1:T(4,128)} %param.36) | copy-start | bytes 388
  31.7 58.4 %reduce-scatter.7.cloned.1.call-start = ((), (), s32[]{:S(2)}) async-start(), calls=%async_computation.5 | async-start | bytes 163840 | tf_op jit(solution)/shard_map/reduce_scatter | solution.py:96
  72.4 46.4 %reduce-scatter.9.cloned.1.call-start = ((), (), s32[]{:S(2)}) async-start(), calls=%async_computation.6 | async-start | bytes 49152 | tf_op jit(solution)/shard_map/reduce_scatter | solution.py:144
  90.1 4.8 %copy-start.1 = (f32[8,4,128,128]{3,2,1,0:T(8,128)S(1)}, f32[8,4,128,128]{3,2,1,0:T(8,128)}, u32[]{:S(2)}) copy-start(f32[8,4,128,128]{3,2,1,0:T(8,128)} %param.38) | copy-start | bytes 6291460
  94.9 4.1 %copy-start.9 = (f32[128]{0:T(128)S(1)}, f32[128]{0:T(128)}, u32[]{:S(2)}) copy-start(f32[128]{0:T(128)} %param.37) | copy-start | bytes 1540
  94.9 17.3 %copy-start.4 = (bf16[512,512]{1,0:T(8,128)(2,1)S(1)}, bf16[512,512]{1,0:T(8,128)(2,1)}, u32[]{:S(2)}) copy-start(bf16[512,512]{1,0:T(8,128)(2,1)} %param.39) | copy-start | bytes 1572868
  94.9 39.1 %copy-start.6 = (f32[2048]{0:T(1024)S(1)}, f32[2048]{0:T(1024)}, u32[]{:S(2)}) copy-start(f32[2048]{0:T(1024)} %param.40) | copy-start | bytes 24580
  95.7 1.3 copy-start.2
  113.0 60.3 %reduce-scatter.11.cloned.1.call-start = ((), (), s32[]{:S(2)}) async-start(), calls=%async_computation.7 | async-start | bytes 147456 | tf_op jit(solution)/shard_map/reduce_scatter | solution.py:152
Sparse Core Ops, SparseCore 0:
  31.8 31.6 reduce-scatter.4
  72.5 17.5 reduce-scatter.6
  113.2 5.6 reduce-scatter.8
  142.0 31.3 reduce-scatter.10
where the time goes:
time: 182 us; the launch traced here: 181 us
  waiting for transfers between devices  69.1 us (38%)
  blocking collectives  59.7 us (33%)
  matrix products  27.2 us (15%)
  between operations  13.9 us (8%)
  other arithmetic  6.18 us (3%)
  local copies, waits for them, and re-layouts  5.02 us (3%)
    reduce_scatter x1, waiting for transfers between devices, shards(): lax.psum_scatter(last_terms.astype(jnp.bfloat16), ('kv', 'tp'), scatter_d...  31.5 us
    reduce_scatter x1, waiting for transfers between devices, shards(): lax.psum_scatter(ffn_terms.astype(jnp.bfloat16), ('kv', 'tp'), scatter_di...  28.7 us
    all_gather x1, blocking collectives, shards(): rows_all = lax.all_gather(tokens, ('kv', 'tp'), axis=1, tiled=True)  16.1 us
    psum x1, blocking collectives, shards(): lax.psum((jnp.sum(first32 * first32, axis=1), jnp.dot(own_scaled, beta_ro...  14.4 us
    all_gather x1, blocking collectives, shards(): rows_last = lax.all_gather(second_rows, ('kv', 'tp'), axis=1, tiled=True)  14.3 us
    all_gather x1, blocking collectives, shards(): lax.all_gather(heads_out, 'kv', axis=0, tiled=True)  13.1 us
    dot_general x2, matrix products, block_terms(): return jnp.dot(hidden, w_down, preferred_element_type=jnp.float32)  9.45 us
    dot_general x2, matrix products, block_terms(): gate_pre = jnp.dot(normed, w_gate, preferred_element_type=jnp.float32)  6.1 us
  transfers between devices with their start and end apart: 4, of which 4 were waited for; matrix products, arithmetic and copies ran while one was open for 2% of the time, Pallas kernels for 0%

commit v1 on v0

--- a/solution.py
+++ b/solution.py
@@ -4,6 +4,11 @@
 from jax.sharding import PartitionSpec as P
 
 EPS = 1e-06
+
+
+def by_each_axis(value, one, other):
+    inner = lax.psum(value, one)
+    return lax.psum(inner, other)
 
 
 def row_scale(values):
@@ -82,13 +87,14 @@
     own_scaled = (first32 * own_gain).astype(jnp.bfloat16)
     beta_rows = lax.dynamic_slice_in_dim(strength_weight, own_block * columns, columns, 0)
     decay_rows = lax.dynamic_slice_in_dim(decay_weight, own_block * columns, columns, 0)
-    squares, beta_pre, decay_logits = lax.psum(
+    squares, beta_pre, decay_logits = by_each_axis(
         (
             jnp.sum(first32 * first32, axis=1),
             jnp.dot(own_scaled, beta_rows, preferred_element_type=jnp.float32),
             jnp.dot(own_scaled, decay_rows, preferred_element_type=jnp.float32),
         ),
-        ("kv", "tp"),
+        "tp",
+        "kv",
     )
     row_factor = lax.rsqrt(squares / model_width + EPS)
     block_gain = lax.dynamic_slice_in_dim(mixer_norm_gain, kv_index * kv_width, kv_width)

time: 182 us -> 182 us (level)
  waiting for transfers between devices: 69.1 us -> 72.2 us
  blocking collectives: 59.7 us -> 56.7 us
    reduce_scatter x1, waiting for transfers between devices: 3 us -> 6.02 us  [shards(): lax.psum_scatter(jnp.concatenate([jnp.dot(block_scaled, weight, preferred...]
    psum x1 -> x2, blocking collectives: 14.4 us -> 11.5 us  [the longest x1 8.94 us: by_each_axis(): return lax.psum(inner, other)]
where the time goes in v1:
time: 182 us; the launch traced here: 181 us
  waiting for transfers between devices  72.2 us (40%)
  blocking collectives  56.7 us (31%)
  matrix products  27.2 us (15%)
  between operations  13.9 us (8%)
  other arithmetic  6.18 us (3%)
  local copies, waits for them, and re-layouts  5.02 us (3%)
    reduce_scatter x1, waiting for transfers between devices, shards(): lax.psum_scatter(last_terms.astype(jnp.bfloat16), ('kv', 'tp'), scatter_d...  31.6 us
    reduce_scatter x1, waiting for transfers between devices, shards(): lax.psum_scatter(ffn_terms.astype(jnp.bfloat16), ('kv', 'tp'), scatter_di...  28.7 us
    all_gather x1, blocking collectives, shards(): rows_all = lax.all_gather(tokens, ('kv', 'tp'), axis=1, tiled=True)  16.1 us
    all_gather x1, blocking collectives, shards(): rows_last = lax.all_gather(second_rows, ('kv', 'tp'), axis=1, tiled=True)  14.2 us
    all_gather x1, blocking collectives, shards(): lax.all_gather(heads_out, 'kv', axis=0, tiled=True)  13.1 us
    dot_general x2, matrix products, block_terms(): return jnp.dot(hidden, w_down, preferred_element_type=jnp.float32)  9.45 us
    psum x1, blocking collectives, by_each_axis(): return lax.psum(inner, other)  8.94 us
    dot_general x2, matrix products, block_terms(): gate_pre = jnp.dot(normed, w_gate, preferred_element_type=jnp.float32)  6.11 us
  transfers between devices with their start and end apart: 4, of which 4 were waited for; matrix products, arithmetic and copies ran while one was open for 2% of the time, Pallas kernels for 0%

profile of v1, /device:TPU:0, one launch (start us, length us, event | category | flops | bytes accessed | tf_op | source)
XLA Modules:
  0.0 181.4 jit_solution(8419079967942011750)
XLA Ops:
  7.2 16.1 %all_gather.12 = bf16[32,2048]{1,0:T(8,128)(2,1)S(1)} all-gather(bf16[32,256]{1,0:T(8,128)(2,1)} %param.22), channel_id=1, replica_groups=mesh['dp'=4,'kv'=4,'tp'=2] {'kv','tp'}, dimensions={1}, use_global_device_ids=true | all-gather | bytes 147456 | tf_op jit(solution)/shard_map/all_gather | solution.py:76
  24.0 3.4 %fusion.26 = f32[32,704]{1,0:T(8,128)} fusion(bf16[2048,704]{0,1:T(8,128)(2,1)} %param.24, bf16[32,2048]{1,0:T(8,128)(2,1)S(1)} %all_gather.12, f32[2048]{0:T(1024)} %param.23, f32[32]{0:T(128)S(1)} %add_rsqrt_fusion.5), kind=kOutput, calls=%fused_computation.41 | convolution fusion | flops 92536832 | bytes 3113088 | tf_op jit(solution)/shard_map/dot_general | solution.py:25
  27.4 4.3 %convolution_convert_fusion.1 = bf16[32,2048]{1,0:T(8,128)(2,1)} fusion(bf16[704,2048]{1,0:T(8,128)(2,1)S(1)} %copy-done, bf16[2048,704]{0,1:T(8,128)(2,1)} %param.25, f32[32,704]{1,0:T(8,128)} %fusion.26, bf16[32,2048]{1,0:T(8,128)(2,1)S(1)} %all_gather.12, f32[2048]{0:T(1024)} %param.23, f32[32]{0:T(128)} %copy-done.8), kind=kOutput, calls=%fused_computation.1 | convolution fusion | flops 185012224 | bytes 6127744 | tf_op jit(solution)/shard_map/dot_general | solution.py:28
  34.8 28.7 %reduce-scatter.5.cloned.1.call-done = bf16[32,256]{1,0:T(8,128)(2,1)} async-done(((bf16[32,2048]{1,0:T(8,128)(2,1)}), bf16[32,256]{1,0:T(8,128)(2,1)}) %reduce-scatter.5.cloned.1.call-update) | async-done | bytes 16400 | tf_op jit(solution)/shard_map/reduce_scatter | solution.py:80
  63.5 0.8 fusion.28
  64.3 1.8 %all_gather.13 = bf16[32,512]{1,0:T(8,128)(2,1)S(1)} all-gather(bf16[32,256]{1,0:T(8,128)(2,1)S(1)} %get-tuple-element.11), channel_id=1, replica_groups=mesh['dp'=4,'kv'=4,'tp'=2] {'tp'}, dimensions={1}, use_global_device_ids=true | all-gather | bytes 49152 | tf_op jit(solution)/shard_map/all_gather | solution.py:85
  67.0 0.8 fusion.41
  68.0 1.2 convolution_convert_fusion.4
  69.2 1.2 convolution_convert_fusion.3
  70.5 1.3 convolution_convert_fusion.6
  72.5 2.5 %all-reduce.1 = (f32[32]{0:T(128)S(1)}, f32[32,8]{0,1:T(8,128)S(1)}, f32[32,8]{0,1:T(8,128)S(1)}) all-reduce(f32[32]{0:T(128)S(1)} %get-tuple-element.10, f32[32,8]{0,1:T(8,128)S(1)} %fusion.43, f32[32,8]{0,1:T(8,128)S(1)} %fusion.41), channel_id=1, replica_groups=mesh['dp'=4,'kv'=4,'tp'=2] {'tp'}, use_global_device_ids=true, to_apply=%region_4.5 | all-reduce | flops 544 | bytes 4352 | tf_op jit(solution)/shard_map/psum | solution.py:10
  75.0 8.9 %all-reduce = (f32[32]{0:T(128)S(1)}, f32[32,8]{0,1:T(8,128)S(1)}, f32[32,8]{0,1:T(8,128)S(1)}) all-reduce(f32[32]{0:T(128)S(1)} %get-tuple-element.7, f32[32,8]{0,1:T(8,128)S(1)} %get-tuple-element.8, f32[32,8]{0,1:T(8,128)S(1)} %get-tuple-element.9), channel_id=1, replica_groups=mesh['dp'=4,'kv'=4,'tp'=2] {'kv'}, use_global_device_ids=true, to_apply=%region_5.6 | all-reduce | flops 544 | bytes 4352 | tf_op jit(solution)/shard_map/psum | solution.py:11
  84.2 6.0 %reduce-scatter.7.cloned.1.call-done = bf16[8,2048]{1,0:T(8,128)(2,1)} async-done(((bf16[32,2048]{1,0:T(8,128)(2,1)}), bf16[8,2048]{1,0:T(8,128)(2,1)}) %reduce-scatter.7.cloned.1.call-update) | async-done | bytes 32784 | tf_op jit(solution)/shard_map/reduce_scatter | solution.py:102
  90.2 1.0 convert_multiply_fusion.4
  91.5 3.4 %fusion.39 = f32[8,4,1,128]{3,2,1,0:T(1,128)S(1)} fusion(f32[8,4,128,128]{3,2,1,0:T(8,128)} %param.38, f32[8,4,128,1]{2,0,1,3:T(8,128)S(1)} %fusion.69), kind=kOutput, calls=%fused_computation.62 | convolution fusion | flops 6291456 | bytes 2129920 | tf_op jit(solution)/shard_map/shd,shde->she/dot_general | solution.py:34
  95.8 1.3 copy-done.2
  97.1 1.9 %fusion.37 = f32[8,4,1,128]{3,2,1,0:T(1,128)S(1)} fusion(f32[8,4,128,128]{3,2,1,0:T(8,128)S(1)} %multiply_add_fusion, f32[8,4,128,1]{2,0,1,3:T(8,128)S(1)} %get-tuple-element.12), kind=kOutput, calls=%fused_computation.60 | convolution fusion | flops 6291456 | bytes 2129920 | tf_op jit(solution)/shard_map/shd,shde->she/dot_general | solution.py:39
  99.2 13.1 %all_gather.14 = bf16[32,512]{1,0:T(8,128)(2,1)S(1)} all-gather(bf16[8,512]{1,0:T(8,128)(2,1)S(1)} %fusion.45), channel_id=1, replica_groups=mesh['dp'=4,'kv'=4,'tp'=2] {'kv'}, dimensions={0}, use_global_device_ids=true | all-gather | bytes 40960 | tf_op jit(solution)/shard_map/all_gather | solution.py:146
  113.2 5.8 %reduce-scatter.9.cloned.1.call-done = bf16[32,256]{1,0:T(8,128)(2,1)} async-done(((bf16[32,512]{1,0:T(8,128)(2,1)}), bf16[32,256]{1,0:T(8,128)(2,1)}) %reduce-scatter.9.cloned.1.call-update) | async-done | bytes 16400 | tf_op jit(solution)/shard_map/reduce_scatter | solution.py:150
  119.7 14.2 %all_gather.15 = bf16[32,2048]{1,0:T(8,128)(2,1)S(1)} all-gather(bf16[32,256]{1,0:T(8,128)(2,1)S(1)} %fusion.30), channel_id=1, replica_groups=mesh['dp'=4,'kv'=4,'tp'=2] {'kv','tp'}, dimensions={1}, use_global_device_ids=true | all-gather | bytes 147456 | tf_op jit(solution)/shard_map/all_gather | solution.py:154
  134.1 2.7 %fusion.22 = f32[32,704]{1,0:T(8,128)S(1)} fusion(bf16[2048,704]{0,1:T(8,128)(2,1)} %param.41, bf16[32,2048]{1,0:T(8,128)(2,1)S(1)} %all_gather.15, f32[2048]{0:T(1024)S(1)} %copy-done.6, f32[32]{0:T(128)S(1)} %add_rsqrt_fusion.3), kind=kOutput, calls=%fused_computation.40 | convolution fusion | flops 92536832 | bytes 3113088 | tf_op jit(solution)/shard_map/dot_general | solution.py:25
  136.8 5.1 %convolution_convert_fusion = bf16[32,2048]{1,0:T(8,128)(2,1)} fusion(bf16[704,2048]{1,0:T(8,128)(2,1)} %param.43, bf16[2048,704]{0,1:T(8,128)(2,1)} %param.42, f32[32,704]{1,0:T(8,128)S(1)} %fusion.22, bf16[32,2048]{1,0:T(8,128)(2,1)S(1)} %all_gather.15, f32[2048]{0:T(1024)S(1)} %copy-done.6, f32[32]{0:T(128)S(1)} %add_rsqrt_fusion.3), kind=kOutput, calls=%fused_computation | convolution fusion | flops 185012224 | bytes 6127744 | tf_op jit(solution)/shard_map/dot_general | solution.py:28
  141.9 31.6 %reduce-scatter.11.cloned.1.call-done = bf16[32,256]{1,0:T(8,128)(2,1)} async-done(((bf16[32,2048]{1,0:T(8,128)(2,1)}), bf16[32,256]{1,0:T(8,128)(2,1)}) %reduce-scatter.11.cloned.1.call-update) | async-done | bytes 16400 | tf_op jit(solution)/shard_map/reduce_scatter | solution.py:158
  173.5 1.3 add_convert_fusion
  (55 shorter events, 8.8 us)
Async XLA Ops:
  7.2 20.2 %copy-start = (bf16[704,2048]{1,0:T(8,128)(2,1)S(1)}, bf16[704,2048]{1,0:T(8,128)(2,1)}, u32[]{:S(2)}) copy-start(bf16[704,2048]{1,0:T(8,128)(2,1)} %param.26) | copy-start | bytes 8650756
  7.2 56.3 %reduce-scatter.5.cloned.1.call-start = ((), (), s32[]{:S(2)}) async-start(), calls=%async_computation.4 | async-start | bytes 147456 | tf_op jit(solution)/shard_map/reduce_scatter | solution.py:80
  23.5 0.5 copy-start.8
  27.4 36.2 %copy-start.5 = (bf16[32,256]{1,0:T(8,128)(2,1)S(1)}, bf16[32,256]{1,0:T(8,128)(2,1)}, u32[]{:S(2)}) copy-start(bf16[32,256]{1,0:T(8,128)(2,1)} %param.22) | copy-start | bytes 49156
  27.4 40.4 %copy-start.3 = (bf16[512,512]{1,0:T(8,128)(2,1)S(1)}, bf16[512,512]{1,0:T(8,128)(2,1)}, u32[]{:S(2)}) copy-start(bf16[512,512]{1,0:T(8,128)(2,1)} %param.29) | copy-start | bytes 1572868
  31.7 52.3 %copy-start.7 = (f32[8,4]{0,1:T(4,128)S(1)}, f32[8,4]{0,1:T(4,128)}, u32[]{:S(2)}) copy-start(f32[8,4]{0,1:T(4,128)} %param.36) | copy-start | bytes 388
  31.7 58.5 %reduce-scatter.7.cloned.1.call-start = ((), (), s32[]{:S(2)}) async-start(), calls=%async_computation.5 | async-start | bytes 163840 | tf_op jit(solution)/shard_map/reduce_scatter | solution.py:102
  72.4 46.6 %reduce-scatter.9.cloned.1.call-start = ((), (), s32[]{:S(2)}) async-start(), calls=%async_computation.6 | async-start | bytes 49152 | tf_op jit(solution)/shard_map/reduce_scatter | solution.py:150
  90.2 4.8 %copy-start.1 = (f32[8,4,128,128]{3,2,1,0:T(8,128)S(1)}, f32[8,4,128,128]{3,2,1,0:T(8,128)}, u32[]{:S(2)}) copy-start(f32[8,4,128,128]{3,2,1,0:T(8,128)} %param.38) | copy-start | bytes 6291460
  95.0 4.1 %copy-start.9 = (f32[128]{0:T(128)S(1)}, f32[128]{0:T(128)}, u32[]{:S(2)}) copy-start(f32[128]{0:T(128)} %param.37) | copy-start | bytes 1540
  95.0 17.3 %copy-start.4 = (bf16[512,512]{1,0:T(8,128)(2,1)S(1)}, bf16[512,512]{1,0:T(8,128)(2,1)}, u32[]{:S(2)}) copy-start(bf16[512,512]{1,0:T(8,128)(2,1)} %param.39) | copy-start | bytes 1572868
  95.0 39.0 %copy-start.6 = (f32[2048]{0:T(1024)S(1)}, f32[2048]{0:T(1024)}, u32[]{:S(2)}) copy-start(f32[2048]{0:T(1024)} %param.40) | copy-start | bytes 24580
  95.8 1.3 copy-start.2
  113.1 60.4 %reduce-scatter.11.cloned.1.call-start = ((), (), s32[]{:S(2)}) async-start(), calls=%async_computation.7 | async-start | bytes 147456 | tf_op jit(solution)/shard_map/reduce_scatter | solution.py:158
Sparse Core Ops, SparseCore 0:
  31.8 31.6 reduce-scatter.4
  72.5 17.6 reduce-scatter.6
  113.3 5.6 reduce-scatter.8
  142.0 31.4 reduce-scatter.10
